TPU v7x, 256 devices: a whole 4x4x8 slice. The times are simulated.
256 devices in a mesh: ep: 32 (over z, x), tp: 8 (over y, core).
Axes of the slice: x: 4, y: 4, z: 8, core: 2. Of those that a mesh axis runs over, the one named last changes fastest.
Arguments:
- stream: bfloat16 [512, 4096], P(None, 'ep'), may hold values from -6.5 to 6.5
- norm_gain: float32 [4096], P('ep'), may hold values from 0.1 to 1.9
- w_query: bfloat16 [4096, 2048], P('ep', 'tp'), may hold values from -0.09375 to 0.09375
- w_key: bfloat16 [4096, 1024], P('ep', 'tp'), may hold values from -0.09375 to 0.09375
- w_value: bfloat16 [4096, 1024], P('ep', 'tp'), may hold values from -0.09375 to 0.09375
- break_offset: float32 [16], P('tp'), may hold values from -10 to -2
- cache_keys: bfloat16 [512, 1024, 8, 128], P('ep', None, 'tp'), may hold values from -6 to 6
- cache_values: bfloat16 [512, 1024, 8, 128], P('ep', None, 'tp'), may hold values from -6 to 6
- lengths: int32 [512], P('ep'), may hold values from 128 to 1024
- w_output: bfloat16 [2048, 4096], P('tp', 'ep'), may hold values from -0.125 to 0.125
- head_gain: float32 [2048], P('tp'), may hold values from 0.1 to 1.9
- ffn_gain: float32 [4096], P('ep'), may hold values from 0.1 to 1.9
- route_experts: int32 [512, 2], replicated, may hold values from 0 to 31, all different within a row; in each aligned block of 512 rows (0 to 511, 512 to 1023, ...) at most 64 rows name the same one
- route_weights: float32 [512, 2], replicated, may hold values from 0.1 to 1
- expert_gate: bfloat16 [32, 4096, 1024], P('ep', None, 'tp'), may hold values from -0.09375 to 0.09375
- expert_up: bfloat16 [32, 4096, 1024], P('ep', None, 'tp'), may hold values from -0.09375 to 0.09375
- expert_down: bfloat16 [32, 1024, 4096], P('ep', 'tp'), may hold values from -0.1875 to 0.1875
- dense_gate: bfloat16 [4096, 4096], P('ep', 'tp'), may hold values from -0.09375 to 0.09375
- dense_up: bfloat16 [4096, 4096], P('ep', 'tp'), may hold values from -0.09375 to 0.09375
- dense_down: bfloat16 [4096, 4096], P('tp', 'ep'), may hold values from -0.09375 to 0.09375
- mix_gain: float32 [4096], P('ep'), may hold values from 0.1 to 1.9
Outputs:
- mixed_out: bfloat16 [512, 4096], P(None, 'ep')
- key_rows: bfloat16 [512, 1024], P('ep', 'tp')
- value_rows: bfloat16 [512, 1024], P('ep', 'tp')
Inputs may be any that keep to these rules, and one draw needn't show every extreme that they name: `route_experts`: in the whole batch no expert is named by more than 64 pairs, a bound that some block reaches; the 2 experts of a token differ.
All inputs are finite; a program needn't handle non-finite values.
Results may differ from a plain program's by a relative error of at most 0.025.
Values may be sent and summed in bfloat16 or wider, within the bound.
A program may use at most 64 MiB of HBM per device.

v0:
```python
import jax
import jax.numpy as jnp
from jax import lax
from jax.sharding import PartitionSpec as P

EPSILON = 1e-06


def sent_to_all(x, axis):
    size = lax.axis_size(axis)
    return lax.all_to_all(jnp.broadcast_to(x[None], (size, *x.shape)), axis, 0, 0, tiled=True)


def taken_together(x, axis):
    return sent_to_all(x, axis).sum(axis=0)


def split_up(x, dim, size):
    lengths = x.shape
    blocks = x.reshape(*lengths[:dim], size, lengths[dim] // size, *lengths[dim + 1 :])
    return jnp.moveaxis(blocks, dim, 0)


def sent_and_summed(x, axis, dim):
    blocks = split_up(x, dim, lax.axis_size(axis))
    arrived = lax.all_to_all(blocks, axis, split_axis=0, concat_axis=0, tiled=True)
    return arrived.astype(jnp.float32).sum(axis=0)


def joined_along(blocks, dim):
    blocks = jnp.moveaxis(blocks, 0, dim)
    lengths = blocks.shape
    return blocks.reshape(*lengths[:dim], lengths[dim] * lengths[dim + 1], *lengths[dim + 2 :])


def gather_directly(x, axis, dim):
    return joined_along(sent_to_all(x, axis), dim)


def of_everyone(x, axis):
    return sent_to_all(x, axis).astype(jnp.float32).sum(axis=0)


def rms_scale(values, gain_vec, model_width):
    squares = taken_together(jnp.sum(values * values, axis=1), "ep")
    return values * lax.rsqrt(squares / model_width + EPSILON)[:, None] * gain_vec[None, :]


def to_heads(normed, weights):
    return sent_and_summed(
        jnp.dot(normed, weights, preferred_element_type=jnp.float32).astype(jnp.bfloat16), "ep", 0
    )


def from_heads(values, weights):
    partial_value = jnp.dot(
        gather_directly(values, "ep", 0), weights, preferred_element_type=jnp.float32
    )
    return (
        of_everyone(partial_value.astype(jnp.bfloat16), "tp")
        .astype(jnp.float32)
        .astype(jnp.bfloat16)
    )


def expert_terms(inputs, gate_w, up_w, down_w):
    gate_val = jnp.einsum("ecd,edf->ecf", inputs, gate_w, preferred_element_type=jnp.float32)
    up_val = jnp.einsum("ecd,edf->ecf", inputs, up_w, preferred_element_type=jnp.float32)
    hidden = (jax.nn.silu(gate_val) * up_val).astype(jnp.bfloat16)
    return jnp.einsum("ecf,efd->ecd", hidden, down_w, preferred_element_type=jnp.float32)


def slot_table(route_experts, experts, capacity):
    chosen = route_experts.reshape(-1)
    onehot = (chosen[:, None] == jnp.arange(experts, dtype=jnp.int32)[None, :]).astype(jnp.int32)
    earlier = jnp.cumsum(onehot, axis=0) - onehot
    rank_in = jnp.sum(earlier * onehot, axis=1)
    slot_ids = chosen * capacity + rank_in
    owners = jnp.arange(chosen.shape[0], dtype=jnp.int32) // route_experts.shape[1]
    filled = (
        jnp.full((experts * capacity,), route_experts.shape[0], jnp.int32).at[slot_ids].set(owners)
    )
    return (slot_ids, filled)


def per_device(
    stream,
    norm_gain,
    w_query,
    w_key,
    w_value,
    break_offset,
    cache_keys,
    cache_values,
    lengths,
    w_output,
    head_gain,
    ffn_gain,
    route_experts,
    route_weights,
    expert_gate,
    expert_up,
    expert_down,
    dense_gate,
    dense_up,
    dense_down,
    mix_gain,
):
    model_width = stream.shape[1] * lax.axis_size("ep")
    block_width = stream.shape[1]
    seq_count = lengths.shape[0]
    kv_local = cache_keys.shape[2]
    head_dim = cache_keys.shape[3]
    heads_local = break_offset.shape[0]
    group_size = heads_local // kv_local
    cache_len = cache_keys.shape[1]
    streamf = stream.astype(jnp.float32)
    normed = rms_scale(streamf, norm_gain, model_width).astype(jnp.bfloat16)
    projected = to_heads(normed, jnp.concatenate([w_query, w_key, w_value], axis=1))
    q_width = w_query.shape[1]
    k_width = w_key.shape[1]
    queries = (
        projected[:, :q_width]
        .astype(jnp.bfloat16)
        .reshape(seq_count, kv_local, group_size, head_dim)
    )
    key_rows = projected[:, q_width : q_width + k_width].astype(jnp.bfloat16)
    value_rows = projected[:, q_width + k_width :].astype(jnp.bfloat16)
    scores = jnp.einsum("skgd,slkd->skgl", queries, cache_keys, preferred_element_type=jnp.float32)
    scores = (
        scores * head_dim ** (-0.5) + break_offset.reshape(kv_local, group_size)[None, :, :, None]
    )
    in_cache = (jnp.arange(cache_len, dtype=jnp.int32)[None, :] < lengths[:, None])[
        :, None, None, :
    ]
    failed = jnp.where(in_cache, jax.nn.log_sigmoid(-scores), 0.0)
    later_sum = lax.cumsum(failed, axis=3, reverse=True) - failed
    weights = jnp.where(in_cache, jnp.exp(jax.nn.log_sigmoid(scores) + later_sum), 0.0).astype(
        jnp.bfloat16
    )
    attended = jnp.einsum(
        "skgl,slkd->skgd", weights, cache_values, preferred_element_type=jnp.float32
    )
    gains = head_gain.reshape(kv_local, group_size, head_dim)[None]
    normalized = (
        attended * lax.rsqrt(jnp.mean(attended * attended, axis=3, keepdims=True) + EPSILON) * gains
    )
    head_out = normalized.astype(jnp.bfloat16).reshape(seq_count, heads_local * head_dim)
    attn_out = from_heads(head_out, w_output)
    residual = streamf + attn_out.astype(jnp.float32)
    normed_ffn = rms_scale(residual, ffn_gain, model_width).astype(jnp.bfloat16)
    dense_width = dense_gate.shape[1]
    gate_up = to_heads(normed_ffn, jnp.concatenate([dense_gate, dense_up], axis=1))
    dense_hidden = (jax.nn.silu(gate_up[:, :dense_width]) * gate_up[:, dense_width:]).astype(
        jnp.bfloat16
    )
    dense_out = from_heads(dense_hidden, dense_down)
    experts = expert_gate.shape[0] * lax.axis_size("ep")
    capacity = 2 * seq_count * route_experts.shape[1] // expert_gate.shape[0]
    slot_ids, filled = slot_table(route_experts, experts, capacity)
    padded = jnp.concatenate([normed_ffn, jnp.zeros((1, block_width), jnp.bfloat16)], axis=0)
    outgoing = padded[filled].reshape(experts, capacity, block_width)
    slot_share = capacity // lax.axis_size("tp")
    own_slots = lax.dynamic_slice_in_dim(outgoing, lax.axis_index("tp") * slot_share, slot_share, 1)
    arrived = lax.all_to_all(own_slots, "ep", split_axis=0, concat_axis=2, tiled=True)
    gathered = lax.all_gather(arrived, "tp", axis=1, tiled=True)
    partial_value = expert_terms(gathered, expert_gate, expert_up, expert_down)
    summed = sent_and_summed(partial_value.astype(jnp.bfloat16), "tp", 1).astype(jnp.bfloat16)
    came_back = lax.all_to_all(summed, "ep", split_axis=2, concat_axis=0, tiled=True)
    returned = gather_directly(came_back, "tp", 1)
    picked = returned.reshape(experts * capacity, block_width)[slot_ids]
    picked = picked.reshape(route_experts.shape[0], route_experts.shape[1], block_width).astype(
        jnp.float32
    )
    shares = route_weights / jnp.sum(route_weights, axis=1, keepdims=True)
    moe_out = jnp.sum(picked * shares[:, :, None], axis=1)
    mixed_out = (residual + moe_out + mix_gain[None, :] * dense_out.astype(jnp.float32)).astype(
        jnp.bfloat16
    )
    return (mixed_out, key_rows, value_rows)


def solution(mesh):
    in_specs = (
        P(None, "ep"),
        P("ep"),
        P("ep", "tp"),
        P("ep", "tp"),
        P("ep", "tp"),
        P("tp"),
        P("ep", None, "tp", None),
        P("ep", None, "tp", None),
        P("ep"),
        P("tp", "ep"),
        P("tp"),
        P("ep"),
        P(),
        P(),
        P("ep", None, "tp"),
        P("ep", None, "tp"),
        P("ep", "tp", None),
        P("ep", "tp"),
        P("ep", "tp"),
        P("tp", "ep"),
        P("ep"),
    )
    out_specs = (P(None, "ep"), P("ep", "tp"), P("ep", "tp"))
    return jax.shard_map(
        per_device, mesh=mesh, in_specs=in_specs, out_specs=out_specs, check_vma=False
    )
```

profile of v0, /device:TPU:1, one launch (start us, length us, event | category | flops | bytes accessed | tf_op | source)
XLA Modules:
  0.0 309.1 jit_solution(11907331791318313063)
XLA Ops:
  1.8 20.5 %all_to_all.85 = f32[32,1,512]{2,1,0:T(1,128)S(1)} all-to-all(f32[32,1,512]{2,1,0:T(1,128)S(1)} %broadcast_in_dim.37), channel_id=1, replica_groups=mesh['ep'=32,'tp'=8] {'ep'}, dimensions={0} | all-to-all | bytes 131072 | tf_op jit(solution)/shard_map/all_to_all | solution.py:11
  24.5 3.9 %all-to-all-start.1 = ((bf16[32,16,512]{2,1,0:T(8,128)(2,1)}), bf16[32,16,512]{2,1,0:T(8,128)(2,1)S(1)}, u32[]{:S(2)}, u32[]{:S(2)}) async-start(bf16[32,16,512]{2,1,0:T(8,128)(2,1)} %bitcast), calls=%async_computation.1 | async-start | bytes 1048576 | tf_op jit(solution)/shard_map/all_to_all | solution.py:26
  29.1 14.2 %all-to-all-done.1 = bf16[32,16,512]{2,1,0:T(8,128)(2,1)S(1)} async-done(((bf16[32,16,512]{2,1,0:T(8,128)(2,1)}), bf16[32,16,512]{2,1,0:T(8,128)(2,1)S(1)}, u32[]{:S(2)}, u32[]{:S(2)}) %all-to-all-start.1) | async-done | bytes 524320 | tf_op jit(solution)/shard_map/all_to_all | solution.py:26
  43.4 3.4 %fusion.32 = (f32[16,2,1024]{2,1,0:T(2,128)S(1)}, f32[16,2,1024]{2,1,0:T(2,128)S(1)}) fusion(pred[16,1024]{1,0:T(8,128)(4,1)S(1)} %iota_compare_fusion.2, f32[2]{0:T(128)} %param.26, bf16[16,2,128]{2,1,0:T(2,128)(2,1)S(1)} %reshape.237, bf16[16,1024,1,128]{3,1,2,0:T(8,128)(2,1)} %param.27), kind=kOutput, calls=%fused_computation.44 | convolution fusion | flops 8716288 | bytes 4481032 | tf_op jit(solution)/shard_map/skgd,slkd->skgl/dot_general | solution.py:129
  47.0 39.6 %reduce-window.14 = f32[16,1,2,8,128]{4,3,2,1,0:T(8,128)S(1)} reduce-window(f32[16,1,2,8,128]{4,3,2,1,0:T(8,128)S(1)} %bitcast.111, f32[]{:T(128)} %constant.52.clone.1), window={size=1x1x1x1x128 pad=0_0x0_0x0_0x0_0x0_127}, to_apply=%region_3.4 | reduce-window | flops 4161536 | bytes 262148 | tf_op jit(solution)/shard_map/reduce-window
  87.1 3.3 %multiply_reduce_fusion.1 = (f32[16,2]{1,0:T(8,128)S(1)}, f32[16,2,128]{2,1,0:T(2,128)S(1)}) fusion(bf16[16,1024,1,128]{3,1,2,0:T(8,128)(2,1)} %param.28, pred[16,1024]{1,0:T(8,128)(4,1)S(1)} %iota_compare_fusion.2, f32[16,2,1024]{2,1,0:T(2,128)S(1)} %reshape.240, f32[16,2,1024]{2,1,0:T(2,128)S(1)} %reshape.243, f32[16,2,1024]{2,1,0:T(2,128)S(1)} %get-tuple-element.6), kind=kOutput, calls=%fused_computation.75 | convolution fusion | flops 9084896 | bytes 4620416 | tf_op jit(solution)/shard_map/skgl,slkd->skgd/dot_general | solution.py:141
  91.3 6.3 %all-to-all-start.2 = ((bf16[32,16,256]{2,1,0:T(8,128)(2,1)}), bf16[32,16,256]{2,1,0:T(8,128)(2,1)S(1)}, u32[]{:S(2)}, u32[]{:S(2)}) async-start(bf16[32,16,256]{2,1,0:T(8,128)(2,1)} %broadcast_in_dim.39), calls=%async_computation.2 | async-start | bytes 524288 | tf_op jit(solution)/shard_map/all_to_all | solution.py:11
  98.0 10.1 %all-to-all-done.2 = bf16[32,16,256]{2,1,0:T(8,128)(2,1)S(1)} async-done(((bf16[32,16,256]{2,1,0:T(8,128)(2,1)}), bf16[32,16,256]{2,1,0:T(8,128)(2,1)S(1)}, u32[]{:S(2)}, u32[]{:S(2)}) %all-to-all-start.2) | async-done | bytes 262176 | tf_op jit(solution)/shard_map/all_to_all | solution.py:11
  109.4 8.2 %all-to-all-start.3 = ((bf16[8,512,128]{2,1,0:T(8,128)(2,1)}), bf16[8,512,128]{2,1,0:T(8,128)(2,1)S(1)}, u32[]{:S(2)}, u32[]{:S(2)}) async-start(bf16[8,512,128]{2,1,0:T(8,128)(2,1)} %broadcast_in_dim.40), calls=%async_computation.3 | async-start | bytes 2097152 | tf_op jit(solution)/shard_map/all_to_all | solution.py:11
  117.8 9.0 %reduce-window.16 = s32[32,8,128]{2,1,0:T(8,128)S(1)} reduce-window(s32[32,8,128]{2,1,0:T(8,128)S(1)} %fusion.43, s32[]{:T(128)} %constant.60.clone.1), window={size=1x1x128 pad=0_0x0_0x127_0}, to_apply=%region_9.10 | reduce-window | flops 4161536 | bytes 262148 | tf_op jit(solution)/shard_map/reduce-window.2
  127.7 4.3 %scatter_custom_fusion = s32[2048]{0:T(1024)S(1)} fusion(s32[1024]{0:T(1024)S(1)} %bitcast.121, s32[1024]{0:T(1024)S(1)} %add_select_fusion, s32[]{:T(128)} %constant.58.clone.1), kind=kCustom, calls=%fused_computation.86 | custom fusion | bytes 8196 | tf_op jit(solution)/shard_map/scatter | solution.py:81
  133.6 3.9 %all-to-all-start.4 = ((f32[32,1,512]{2,1,0:T(1,128)}), f32[32,1,512]{2,1,0:T(1,128)S(1)}, u32[]{:S(2)}, u32[]{:S(2)}) async-start(f32[32,1,512]{2,1,0:T(1,128)} %broadcast_in_dim.41), calls=%async_computation.4 | async-start | bytes 131072 | tf_op jit(solution)/shard_map/all_to_all | solution.py:11
  137.4 8.9 %all-to-all-done.4 = f32[32,1,512]{2,1,0:T(1,128)S(1)} async-done(((f32[32,1,512]{2,1,0:T(1,128)}), f32[32,1,512]{2,1,0:T(1,128)S(1)}, u32[]{:S(2)}, u32[]{:S(2)}) %all-to-all-start.4) | async-done | bytes 65568 | tf_op jit(solution)/shard_map/all_to_all | solution.py:11
  146.5 6.2 %gather_fusion = bf16[2048,128]{1,0:T(8,128)(2,1)S(1)} fusion(bf16[513,128]{1,0:T(8,128)(2,1)S(1)} %concatenate.10, s32[2048]{0:T(1024)S(1)} %fusion.52), kind=kCustom, calls=%fused_computation | custom fusion | bytes 1056768 | tf_op jit(solution)/shard_map/gather | solution.py:162
  152.8 12.0 %all_to_all.86 = bf16[32,8,128]{2,1,0:T(8,128)(2,1)S(1)} all-to-all(bf16[32,8,128]{2,1,0:T(8,128)(2,1)S(1)} %constant_dynamic-slice_fusion), channel_id=1, replica_groups=mesh['ep'=32,'tp'=8] {'ep'}, dimensions={0} | all-to-all | bytes 131072 | tf_op jit(solution)/shard_map/all_to_all | solution.py:165
  164.8 16.2 %all_gather.3 = bf16[1,64,4096]{2,1,0:T(8,128)(2,1)S(1)} all-gather(bf16[1,8,4096]{2,1,0:T(8,128)(2,1)S(1)} %bitcast.112), channel_id=1, replica_groups=mesh['ep'=32,'tp'=8] {'tp'}, dimensions={1}, use_global_device_ids=true | all-gather | bytes 589824 | tf_op jit(solution)/shard_map/all_gather | solution.py:166
  183.9 3.6 %all-to-all-start.6 = ((bf16[8,1,8,4096]{3,2,1,0:T(8,128)(2,1)}), bf16[8,1,8,4096]{3,2,1,0:T(8,128)(2,1)S(1)}, u32[]{:S(2)}, u32[]{:S(2)}) async-start(bf16[8,1,8,4096]{3,2,1,0:T(8,128)(2,1)} %fusion), calls=%async_computation.6 | async-start | bytes 1048576 | tf_op jit(solution)/shard_map/all_to_all | solution.py:26
  188.9 8.0 %all-to-all-done.6 = bf16[8,1,8,4096]{3,2,1,0:T(8,128)(2,1)S(1)} async-done(((bf16[8,1,8,4096]{3,2,1,0:T(8,128)(2,1)}), bf16[8,1,8,4096]{3,2,1,0:T(8,128)(2,1)S(1)}, u32[]{:S(2)}, u32[]{:S(2)}) %all-to-all-start.6) | async-done | bytes 524320 | tf_op jit(solution)/shard_map/all_to_all | solution.py:26
  196.9 4.8 %all-to-all-start.9 = ((bf16[32,16,1024]{2,1,0:T(8,128)(2,1)}), bf16[32,16,1024]{2,1,0:T(8,128)(2,1)}, u32[]{:S(2)}, u32[]{:S(2)}) async-start(bf16[32,16,1024]{2,1,0:T(8,128)(2,1)} %bitcast.28), calls=%async_computation.9 | async-start | bytes 2097152 | tf_op jit(solution)/shard_map/all_to_all | solution.py:26
  205.1 23.4 %reduce.9 = bf16[4096,8]{1,0:T(8,128)(2,1)} reduce(bf16[4096,1,8]{2,1,0:T(2,128)(2,1)S(1)} %bitcast.103, bf16[]{:T(256)} %broadcast.165), dimensions={1}, to_apply=%bitcast.86.reduce_sub_computation | reduce | bytes 131074
  228.5 3.1 reshape.282
  231.6 9.1 %all-to-all-start.7 = ((bf16[32,2,512]{2,1,0:T(2,128)(2,1)}), bf16[32,2,512]{2,1,0:T(2,128)(2,1)S(1)}, u32[]{:S(2)}, u32[]{:S(2)}) async-start(bf16[32,2,512]{2,1,0:T(2,128)(2,1)} %reshape.282), calls=%async_computation.7 | async-start | bytes 131072 | tf_op jit(solution)/shard_map/all_to_all | solution.py:169
  242.2 7.4 %all-to-all-done.7 = bf16[32,2,512]{2,1,0:T(2,128)(2,1)S(1)} async-done(((bf16[32,2,512]{2,1,0:T(2,128)(2,1)}), bf16[32,2,512]{2,1,0:T(2,128)(2,1)S(1)}, u32[]{:S(2)}, u32[]{:S(2)}) %all-to-all-start.7) | async-done | bytes 65568 | tf_op jit(solution)/shard_map/all_to_all | solution.py:169
  250.4 4.6 %all-to-all-start.10 = ((bf16[32,16,512]{2,1,0:T(8,128)(2,1)}), bf16[32,16,512]{2,1,0:T(8,128)(2,1)}, u32[]{:S(2)}, u32[]{:S(2)}) async-start(bf16[32,16,512]{2,1,0:T(8,128)(2,1)} %broadcast_in_dim.46), calls=%async_computation.10 | async-start | bytes 1048576 | tf_op jit(solution)/shard_map/all_to_all | solution.py:11
  255.1 2.8 reshape.283
  259.8 9.4 %all-to-all-done.10 = bf16[32,16,512]{2,1,0:T(8,128)(2,1)} async-done(((bf16[32,16,512]{2,1,0:T(8,128)(2,1)}), bf16[32,16,512]{2,1,0:T(8,128)(2,1)}, u32[]{:S(2)}, u32[]{:S(2)}) %all-to-all-start.10) | async-done | bytes 524320 | tf_op jit(solution)/shard_map/all_to_all | solution.py:11
  270.1 8.2 %all-to-all-start.8 = ((bf16[8,32,8,128]{3,2,1,0:T(8,128)(2,1)}), bf16[8,32,8,128]{3,2,1,0:T(8,128)(2,1)S(1)}, u32[]{:S(2)}, u32[]{:S(2)}) async-start(bf16[8,32,8,128]{3,2,1,0:T(8,128)(2,1)} %broadcast_in_dim.45), calls=%async_computation.8 | async-start | bytes 1048576 | tf_op jit(solution)/shard_map/all_to_all | solution.py:11
  279.6 8.0 %all-to-all-done.8 = bf16[8,32,8,128]{3,2,1,0:T(8,128)(2,1)S(1)} async-done(((bf16[8,32,8,128]{3,2,1,0:T(8,128)(2,1)}), bf16[8,32,8,128]{3,2,1,0:T(8,128)(2,1)S(1)}, u32[]{:S(2)}, u32[]{:S(2)}) %all-to-all-start.8) | async-done | bytes 524320 | tf_op jit(solution)/shard_map/all_to_all | solution.py:11
  288.8 4.4 %all-to-all-start.11 = ((bf16[8,512,128]{2,1,0:T(8,128)(2,1)}), bf16[8,512,128]{2,1,0:T(8,128)(2,1)S(1)}, u32[]{:S(2)}, u32[]{:S(2)}) async-start(bf16[8,512,128]{2,1,0:T(8,128)(2,1)} %broadcast_in_dim.47), calls=%async_computation.11 | async-start | bytes 2097152 | tf_op jit(solution)/shard_map/all_to_all | solution.py:11
  294.9 3.2 %gather_fusion.1 = bf16[1024,128]{1,0:T(8,128)(2,1)S(1)} fusion(bf16[2048,128]{1,0:T(8,128)(2,1)S(1)} %bitcast.102, s32[1024]{0:T(1024)S(1)} %broadcast_clamp_fusion), kind=kCustom, calls=%fused_computation.1 | custom fusion | bytes 528384 | tf_op jit(solution)/shard_map/gather | solution.py:171
  298.1 3.7 %fusion.17 = f32[512,128]{1,0:T(8,128)S(1)} fusion(bf16[512,2,128]{2,1,0:T(2,128)(2,1)S(1)} %bitcast.107, f32[512,2]{1,0:T(8,128)} %copy.90), kind=kLoop, calls=%fused_computation.23 | loop fusion | flops 327680 | bytes 528384 | tf_op jit(solution)/shard_map/reduce_sum | solution.py:176
  301.8 6.4 %all-to-all-done.11 = bf16[8,512,128]{2,1,0:T(8,128)(2,1)S(1)} async-done(((bf16[8,512,128]{2,1,0:T(8,128)(2,1)}), bf16[8,512,128]{2,1,0:T(8,128)(2,1)S(1)}, u32[]{:S(2)}, u32[]{:S(2)}) %all-to-all-start.11) | async-done | bytes 1048608 | tf_op jit(solution)/shard_map/all_to_all | solution.py:11
  (95 shorter events, 27.9 us)
Async XLA Ops:
  0.6 181.9 %copy-start = (bf16[1,128,4096]{2,1,0:T(8,128)(2,1)S(1)}, bf16[1,128,4096]{2,1,0:T(8,128)(2,1)}, u32[]{:S(2)}) copy-start(bf16[1,128,4096]{2,1,0:T(8,128)(2,1)} %param.37) | copy-start | bytes 3145732
  24.5 18.8 %all-to-all-start.1 = ((bf16[32,16,512]{2,1,0:T(8,128)(2,1)}), bf16[32,16,512]{2,1,0:T(8,128)(2,1)S(1)}, u32[]{:S(2)}, u32[]{:S(2)}) async-start(bf16[32,16,512]{2,1,0:T(8,128)(2,1)} %bitcast), calls=%async_computation.1 | async-start | bytes 1048576 | tf_op jit(solution)/shard_map/all_to_all | solution.py:26
  46.8 43.6 %copy-start.8 = (f32[256]{0:T(256)S(1)}, f32[256]{0:T(256)}, u32[]{:S(2)}) copy-start(f32[256]{0:T(256)} %param.31) | copy-start | bytes 3076
  46.8 50.8 %copy-start.6 = (s32[512,2]{0,1:T(2,128)S(1)}, s32[512,2]{0,1:T(2,128)}, u32[]{:S(2)}) copy-start(s32[512,2]{0,1:T(2,128)} %param.33) | copy-start | bytes 12292
  46.9 61.1 %copy-start.5 = (bf16[256,128]{1,0:T(8,128)(2,1)S(1)}, bf16[256,128]{1,0:T(8,128)(2,1)}, u32[]{:S(2)}) copy-start(bf16[256,128]{1,0:T(8,128)(2,1)} %param.30) | copy-start | bytes 196612
  90.5 42.2 %copy-start.1 = (bf16[512,128]{1,0:T(8,128)(2,1)S(1)}, bf16[512,128]{1,0:T(8,128)(2,1)}, u32[]{:S(2)}) copy-start(bf16[512,128]{1,0:T(8,128)(2,1)} %param.21) | copy-start | bytes 393220
  91.3 55.1 %copy-start.9 = (f32[128]{0:T(128)S(1)}, f32[128]{0:T(128)}, u32[]{:S(2)}) copy-start(f32[128]{0:T(128)} %param.32) | copy-start | bytes 1540
  91.3 16.7 %all-to-all-start.2 = ((bf16[32,16,256]{2,1,0:T(8,128)(2,1)}), bf16[32,16,256]{2,1,0:T(8,128)(2,1)S(1)}, u32[]{:S(2)}, u32[]{:S(2)}) async-start(bf16[32,16,256]{2,1,0:T(8,128)(2,1)} %broadcast_in_dim.39), calls=%async_computation.2 | async-start | bytes 524288 | tf_op jit(solution)/shard_map/all_to_all | solution.py:11
  109.4 23.2 %all-to-all-start.3 = ((bf16[8,512,128]{2,1,0:T(8,128)(2,1)}), bf16[8,512,128]{2,1,0:T(8,128)(2,1)S(1)}, u32[]{:S(2)}, u32[]{:S(2)}) async-start(bf16[8,512,128]{2,1,0:T(8,128)(2,1)} %broadcast_in_dim.40), calls=%async_computation.3 | async-start | bytes 2097152 | tf_op jit(solution)/shard_map/all_to_all | solution.py:11
  132.7 49.8 %copy-start.2 = (bf16[1,4096,128]{2,1,0:T(8,128)(2,1)S(1)}, bf16[1,4096,128]{2,1,0:T(8,128)(2,1)}, u32[]{:S(2)}) copy-start(bf16[1,4096,128]{2,1,0:T(8,128)(2,1)} %param.36) | copy-start | bytes 3145732
  133.6 12.7 %all-to-all-start.4 = ((f32[32,1,512]{2,1,0:T(1,128)}), f32[32,1,512]{2,1,0:T(1,128)S(1)}, u32[]{:S(2)}, u32[]{:S(2)}) async-start(f32[32,1,512]{2,1,0:T(1,128)} %broadcast_in_dim.41), calls=%async_computation.4 | async-start | bytes 131072 | tf_op jit(solution)/shard_map/all_to_all | solution.py:11
  152.7 34.8 %copy-start.3 = (bf16[128,512]{1,0:T(8,128)(2,1)S(1)}, bf16[128,512]{1,0:T(8,128)(2,1)}, u32[]{:S(2)}) copy-start(bf16[128,512]{1,0:T(8,128)(2,1)} %param.39) | copy-start | bytes 393220
  152.7 34.8 %copy-start.4 = (bf16[128,512]{1,0:T(8,128)(2,1)S(1)}, bf16[128,512]{1,0:T(8,128)(2,1)}, u32[]{:S(2)}) copy-start(bf16[128,512]{1,0:T(8,128)(2,1)} %param.38) | copy-start | bytes 393220
  183.9 12.9 %all-to-all-start.6 = ((bf16[8,1,8,4096]{3,2,1,0:T(8,128)(2,1)}), bf16[8,1,8,4096]{3,2,1,0:T(8,128)(2,1)S(1)}, u32[]{:S(2)}, u32[]{:S(2)}) async-start(bf16[8,1,8,4096]{3,2,1,0:T(8,128)(2,1)} %fusion), calls=%async_computation.6 | async-start | bytes 1048576 | tf_op jit(solution)/shard_map/all_to_all | solution.py:26
  196.9 34.7 %all-to-all-start.9 = ((bf16[32,16,1024]{2,1,0:T(8,128)(2,1)}), bf16[32,16,1024]{2,1,0:T(8,128)(2,1)}, u32[]{:S(2)}, u32[]{:S(2)}) async-start(bf16[32,16,1024]{2,1,0:T(8,128)(2,1)} %bitcast.28), calls=%async_computation.9 | async-start | bytes 2097152 | tf_op jit(solution)/shard_map/all_to_all | solution.py:26
  231.6 18.0 %all-to-all-start.7 = ((bf16[32,2,512]{2,1,0:T(2,128)(2,1)}), bf16[32,2,512]{2,1,0:T(2,128)(2,1)S(1)}, u32[]{:S(2)}, u32[]{:S(2)}) async-start(bf16[32,2,512]{2,1,0:T(2,128)(2,1)} %reshape.282), calls=%async_computation.7 | async-start | bytes 131072 | tf_op jit(solution)/shard_map/all_to_all | solution.py:169
  250.4 18.8 %all-to-all-start.10 = ((bf16[32,16,512]{2,1,0:T(8,128)(2,1)}), bf16[32,16,512]{2,1,0:T(8,128)(2,1)}, u32[]{:S(2)}, u32[]{:S(2)}) async-start(bf16[32,16,512]{2,1,0:T(8,128)(2,1)} %broadcast_in_dim.46), calls=%async_computation.10 | async-start | bytes 1048576 | tf_op jit(solution)/shard_map/all_to_all | solution.py:11
  257.9 35.4 %copy-start.7 = (f32[512,2]{0,1:T(2,128)S(1)}, f32[512,2]{0,1:T(2,128)}, u32[]{:S(2)}) copy-start(f32[512,2]{0,1:T(2,128)} %param.34) | copy-start | bytes 12292
  270.1 17.6 %all-to-all-start.8 = ((bf16[8,32,8,128]{3,2,1,0:T(8,128)(2,1)}), bf16[8,32,8,128]{3,2,1,0:T(8,128)(2,1)S(1)}, u32[]{:S(2)}, u32[]{:S(2)}) async-start(bf16[8,32,8,128]{3,2,1,0:T(8,128)(2,1)} %broadcast_in_dim.45), calls=%async_computation.8 | async-start | bytes 1048576 | tf_op jit(solution)/shard_map/all_to_all | solution.py:11
  279.6 28.7 %copy-start.10 = (f32[128]{0:T(128)S(1)}, f32[128]{0:T(128)}, u32[]{:S(2)}) copy-start(f32[128]{0:T(128)} %param.41) | copy-start | bytes 1540
  288.8 19.4 %all-to-all-start.11 = ((bf16[8,512,128]{2,1,0:T(8,128)(2,1)}), bf16[8,512,128]{2,1,0:T(8,128)(2,1)S(1)}, u32[]{:S(2)}, u32[]{:S(2)}) async-start(bf16[8,512,128]{2,1,0:T(8,128)(2,1)} %broadcast_in_dim.47), calls=%async_computation.11 | async-start | bytes 2097152 | tf_op jit(solution)/shard_map/all_to_all | solution.py:11
where the time goes:
time: 310 us; the launch traced here: 309 us
  other arithmetic  81 us (26%)
  waiting for transfers between devices  72.8 us (23%)
  starting transfers between devices  57.1 us (18%)
  blocking collectives  48.7 us (16%)
  local copies, waits for them, and re-layouts  33.7 us (11%)
  matrix products  14.7 us (5%)
    another operation x5, other arithmetic  48.8 us
    all_to_all x6, waiting for transfers between devices, sent_to_all(): lax.all_to_all(jnp.broadcast_to(x[None], (size, *x.shape)), axis, 0, 0, t...  43.3 us
    all_to_all x6, starting transfers between devices, sent_to_all(): lax.all_to_all(jnp.broadcast_to(x[None], (size, *x.shape)), axis, 0, 0, t...  35.6 us
    unnamed x1, other arithmetic  23.4 us
    all_to_all x3, waiting for transfers between devices, sent_and_summed(): lax.all_to_all(blocks, axis, split_axis=0, concat_axis=0, tiled=True)  22.1 us
    all_to_all x1, blocking collectives, sent_to_all(): lax.all_to_all(jnp.broadcast_to(x[None], (size, *x.shape)), axis, 0, 0, t...  20.5 us
    all_gather x1, blocking collectives, per_device(): gathered = lax.all_gather(arrived, 'tp', axis=1, tiled=True)  16.2 us
    all_to_all x3, starting transfers between devices, sent_and_summed(): lax.all_to_all(blocks, axis, split_axis=0, concat_axis=0, tiled=True)  12.3 us
  transfers between devices with their start and end apart: 10, of which 9 were waited for; matrix products, arithmetic and copies ran while one was open for 20% of the time, Pallas kernels for 0%

commit v1 on v0

--- a/solution.py
+++ b/solution.py
@@ -163,7 +163,11 @@
     slot_share = capacity // lax.axis_size("tp")
     own_slots = lax.dynamic_slice_in_dim(outgoing, lax.axis_index("tp") * slot_share, slot_share, 1)
     arrived = lax.all_to_all(own_slots, "ep", split_axis=0, concat_axis=2, tiled=True)
-    gathered = lax.all_gather(arrived, "tp", axis=1, tiled=True)
+    size_2 = lax.axis_size("tp")
+    repeats = [size_2 if d == 1 else 1 for d in range(arrived.ndim)]
+    gathered = lax.all_to_all(
+        jnp.tile(arrived, repeats), "tp", split_axis=1, concat_axis=1, tiled=True
+    )
     partial_value = expert_terms(gathered, expert_gate, expert_up, expert_down)
     summed = sent_and_summed(partial_value.astype(jnp.bfloat16), "tp", 1).astype(jnp.bfloat16)
     came_back = lax.all_to_all(summed, "ep", split_axis=2, concat_axis=0, tiled=True)

time: 310 us -> 319 us (1.029)
  other arithmetic: 81 us -> 84.8 us
    all_gather x1 -> x0, blocking collectives: 16.2 us -> none  [per_device(): gathered = lax.all_gather(arrived, 'tp', axis=1, tiled=True)]
    all_to_all x0 -> x1, blocking collectives: none -> 15.8 us  [per_device(): lax.all_to_all(jnp.tile(arrived, repeats), 'tp', split_axis=1, concat_axi...]
    unnamed x1 -> x2, other arithmetic: 23.4 us -> 27.2 us
where the time goes in v1:
time: 319 us; the launch traced here: 317 us
  other arithmetic  84.8 us (27%)
  waiting for transfers between devices  72.8 us (23%)
  starting transfers between devices  57.8 us (18%)
  blocking collectives  48.2 us (15%)
  local copies, waits for them, and re-layouts  35.9 us (11%)
  matrix products  16.8 us (5%)
    another operation x5, other arithmetic  48.8 us
    all_to_all x6, waiting for transfers between devices, sent_to_all(): lax.all_to_all(jnp.broadcast_to(x[None], (size, *x.shape)), axis, 0, 0, t...  43.3 us
    all_to_all x6, starting transfers between devices, sent_to_all(): lax.all_to_all(jnp.broadcast_to(x[None], (size, *x.shape)), axis, 0, 0, t...  35.6 us
    unnamed x2, other arithmetic  27.2 us
    all_to_all x3, waiting for transfers between devices, sent_and_summed(): lax.all_to_all(blocks, axis, split_axis=0, concat_axis=0, tiled=True)  22.1 us
    all_to_all x1, blocking collectives, sent_to_all(): lax.all_to_all(jnp.broadcast_to(x[None], (size, *x.shape)), axis, 0, 0, t...  20.5 us
    all_to_all x1, blocking collectives, per_device(): lax.all_to_all(jnp.tile(arrived, repeats), 'tp', split_axis=1, concat_axi...  15.8 us
    all_to_all x3, starting transfers between devices, sent_and_summed(): lax.all_to_all(blocks, axis, split_axis=0, concat_axis=0, tiled=True)  13.2 us
  transfers between devices with their start and end apart: 10, of which 9 were waited for; matrix products, arithmetic and copies ran while one was open for 20% of the time, Pallas kernels for 0%

profile of v1, /device:TPU:1, one launch (start us, length us, event | category | flops | bytes accessed | tf_op | source)
XLA Modules:
  0.0 317.4 jit_solution(1583011930982867396)
XLA Ops:
  1.8 20.5 %all_to_all.87 = f32[32,1,512]{2,1,0:T(1,128)S(1)} all-to-all(f32[32,1,512]{2,1,0:T(1,128)S(1)} %broadcast_in_dim.37), channel_id=1, replica_groups=mesh['ep'=32,'tp'=8] {'ep'}, dimensions={0} | all-to-all | bytes 131072 | tf_op jit(solution)/shard_map/all_to_all | solution.py:11
  24.5 3.9 %all-to-all-start.1 = ((bf16[32,16,512]{2,1,0:T(8,128)(2,1)}), bf16[32,16,512]{2,1,0:T(8,128)(2,1)S(1)}, u32[]{:S(2)}, u32[]{:S(2)}) async-start(bf16[32,16,512]{2,1,0:T(8,128)(2,1)} %bitcast), calls=%async_computation.1 | async-start | bytes 1048576 | tf_op jit(solution)/shard_map/all_to_all | solution.py:26
  29.1 14.2 %all-to-all-done.1 = bf16[32,16,512]{2,1,0:T(8,128)(2,1)S(1)} async-done(((bf16[32,16,512]{2,1,0:T(8,128)(2,1)}), bf16[32,16,512]{2,1,0:T(8,128)(2,1)S(1)}, u32[]{:S(2)}, u32[]{:S(2)}) %all-to-all-start.1) | async-done | bytes 524320 | tf_op jit(solution)/shard_map/all_to_all | solution.py:26
  43.4 3.4 %fusion.35 = (f32[16,2,1024]{2,1,0:T(2,128)S(1)}, f32[16,2,1024]{2,1,0:T(2,128)S(1)}) fusion(pred[16,1024]{1,0:T(8,128)(4,1)S(1)} %iota_compare_fusion.2, f32[2]{0:T(128)} %param.26, bf16[16,2,128]{2,1,0:T(2,128)(2,1)S(1)} %reshape.244, bf16[16,1024,1,128]{3,1,2,0:T(8,128)(2,1)} %param.27), kind=kOutput, calls=%fused_computation.47 | convolution fusion | flops 8716288 | bytes 4481032 | tf_op jit(solution)/shard_map/skgd,slkd->skgl/dot_general | solution.py:129
  47.0 39.6 %reduce-window.14 = f32[16,1,2,8,128]{4,3,2,1,0:T(8,128)S(1)} reduce-window(f32[16,1,2,8,128]{4,3,2,1,0:T(8,128)S(1)} %bitcast.120, f32[]{:T(128)} %constant.52.clone.1), window={size=1x1x1x1x128 pad=0_0x0_0x0_0x0_0x0_127}, to_apply=%region_3.4 | reduce-window | flops 4161536 | bytes 262148 | tf_op jit(solution)/shard_map/reduce-window
  87.1 3.3 %multiply_reduce_fusion.1 = (f32[16,2]{1,0:T(8,128)S(1)}, f32[16,2,128]{2,1,0:T(2,128)S(1)}) fusion(bf16[16,1024,1,128]{3,1,2,0:T(8,128)(2,1)} %param.28, pred[16,1024]{1,0:T(8,128)(4,1)S(1)} %iota_compare_fusion.2, f32[16,2,1024]{2,1,0:T(2,128)S(1)} %reshape.247, f32[16,2,1024]{2,1,0:T(2,128)S(1)} %reshape.250, f32[16,2,1024]{2,1,0:T(2,128)S(1)} %get-tuple-element.6), kind=kOutput, calls=%fused_computation.78 | convolution fusion | flops 9084896 | bytes 4620416 | tf_op jit(solution)/shard_map/skgl,slkd->skgd/dot_general | solution.py:141
  91.3 6.3 %all-to-all-start.2 = ((bf16[32,16,256]{2,1,0:T(8,128)(2,1)}), bf16[32,16,256]{2,1,0:T(8,128)(2,1)S(1)}, u32[]{:S(2)}, u32[]{:S(2)}) async-start(bf16[32,16,256]{2,1,0:T(8,128)(2,1)} %broadcast_in_dim.39), calls=%async_computation.2 | async-start | bytes 524288 | tf_op jit(solution)/shard_map/all_to_all | solution.py:11
  98.0 10.1 %all-to-all-done.2 = bf16[32,16,256]{2,1,0:T(8,128)(2,1)S(1)} async-done(((bf16[32,16,256]{2,1,0:T(8,128)(2,1)}), bf16[32,16,256]{2,1,0:T(8,128)(2,1)S(1)}, u32[]{:S(2)}, u32[]{:S(2)}) %all-to-all-start.2) | async-done | bytes 262176 | tf_op jit(solution)/shard_map/all_to_all | solution.py:11
  109.4 8.2 %all-to-all-start.3 = ((bf16[8,512,128]{2,1,0:T(8,128)(2,1)}), bf16[8,512,128]{2,1,0:T(8,128)(2,1)S(1)}, u32[]{:S(2)}, u32[]{:S(2)}) async-start(bf16[8,512,128]{2,1,0:T(8,128)(2,1)} %broadcast_in_dim.40), calls=%async_computation.3 | async-start | bytes 2097152 | tf_op jit(solution)/shard_map/all_to_all | solution.py:11
  117.8 9.0 %reduce-window.16 = s32[32,8,128]{2,1,0:T(8,128)S(1)} reduce-window(s32[32,8,128]{2,1,0:T(8,128)S(1)} %fusion.46, s32[]{:T(128)} %constant.60.clone.1), window={size=1x1x128 pad=0_0x0_0x127_0}, to_apply=%region_9.10 | reduce-window | flops 4161536 | bytes 262148 | tf_op jit(solution)/shard_map/reduce-window.2
  127.7 4.3 %scatter_custom_fusion = s32[2048]{0:T(1024)S(1)} fusion(s32[1024]{0:T(1024)S(1)} %bitcast.130, s32[1024]{0:T(1024)S(1)} %add_select_fusion, s32[]{:T(128)} %constant.58.clone.1), kind=kCustom, calls=%fused_computation.89 | custom fusion | bytes 8196 | tf_op jit(solution)/shard_map/scatter | solution.py:81
  133.5 3.9 %all-to-all-start.4 = ((f32[32,1,512]{2,1,0:T(1,128)}), f32[32,1,512]{2,1,0:T(1,128)S(1)}, u32[]{:S(2)}, u32[]{:S(2)}) async-start(f32[32,1,512]{2,1,0:T(1,128)} %broadcast_in_dim.41), calls=%async_computation.4 | async-start | bytes 131072 | tf_op jit(solution)/shard_map/all_to_all | solution.py:11
  137.4 8.9 %all-to-all-done.4 = f32[32,1,512]{2,1,0:T(1,128)S(1)} async-done(((f32[32,1,512]{2,1,0:T(1,128)}), f32[32,1,512]{2,1,0:T(1,128)S(1)}, u32[]{:S(2)}, u32[]{:S(2)}) %all-to-all-start.4) | async-done | bytes 65568 | tf_op jit(solution)/shard_map/all_to_all | solution.py:11
  146.5 6.2 %gather_fusion = bf16[2048,128]{1,0:T(8,128)(2,1)S(1)} fusion(bf16[513,128]{1,0:T(8,128)(2,1)S(1)} %concatenate.10, s32[2048]{0:T(1024)S(1)} %fusion.55), kind=kCustom, calls=%fused_computation | custom fusion | bytes 1056768 | tf_op jit(solution)/shard_map/gather | solution.py:162
  152.8 11.9 %all_to_all.88 = bf16[32,8,128]{2,1,0:T(8,128)(2,1)S(1)} all-to-all(bf16[32,8,128]{2,1,0:T(8,128)(2,1)S(1)} %constant_dynamic-slice_fusion), channel_id=1, replica_groups=mesh['ep'=32,'tp'=8] {'ep'}, dimensions={0} | all-to-all | bytes 131072 | tf_op jit(solution)/shard_map/all_to_all | solution.py:165
  166.3 3.8 %reduce.9 = bf16[64,4096]{1,0:T(8,128)(2,1)S(1)} reduce(bf16[64,1,4096]{2,1,0:T(2,128)(2,1)S(1)} %bitcast.113, bf16[]{:T(256)} %broadcast.168), dimensions={1}, to_apply=%bitcast.106.reduce_sub_computation | reduce | bytes 1048578
  170.7 15.8 %all_to_all.89 = bf16[8,2,16384]{2,1,0:T(2,128)(2,1)S(1)} all-to-all(bf16[8,2,16384]{2,1,0:T(2,128)(2,1)S(1)} %reshape.289), channel_id=1, replica_groups=mesh['ep'=32,'tp'=8] {'tp'}, dimensions={0} | all-to-all | bytes 1048576 | tf_op jit(solution)/shard_map/all_to_all | solution.py:168
  192.1 4.4 %all-to-all-start.7 = ((bf16[8,1,8,4096]{3,2,1,0:T(8,128)(2,1)}), bf16[8,1,8,4096]{3,2,1,0:T(8,128)(2,1)S(1)}, u32[]{:S(2)}, u32[]{:S(2)}) async-start(bf16[8,1,8,4096]{3,2,1,0:T(8,128)(2,1)} %fusion), calls=%async_computation.7 | async-start | bytes 1048576 | tf_op jit(solution)/shard_map/all_to_all | solution.py:26
  197.9 8.0 %all-to-all-done.7 = bf16[8,1,8,4096]{3,2,1,0:T(8,128)(2,1)S(1)} async-done(((bf16[8,1,8,4096]{3,2,1,0:T(8,128)(2,1)}), bf16[8,1,8,4096]{3,2,1,0:T(8,128)(2,1)S(1)}, u32[]{:S(2)}, u32[]{:S(2)}) %all-to-all-start.7) | async-done | bytes 524320 | tf_op jit(solution)/shard_map/all_to_all | solution.py:26
  205.9 4.9 %all-to-all-start.10 = ((bf16[32,16,1024]{2,1,0:T(8,128)(2,1)}), bf16[32,16,1024]{2,1,0:T(8,128)(2,1)}, u32[]{:S(2)}, u32[]{:S(2)}) async-start(bf16[32,16,1024]{2,1,0:T(8,128)(2,1)} %bitcast.28), calls=%async_computation.10 | async-start | bytes 2097152 | tf_op jit(solution)/shard_map/all_to_all | solution.py:26
  213.6 23.4 %reduce.10 = bf16[4096,8]{1,0:T(8,128)(2,1)} reduce(bf16[4096,1,8]{2,1,0:T(2,128)(2,1)S(1)} %bitcast.109, bf16[]{:T(256)} %broadcast.168), dimensions={1}, to_apply=%bitcast.90.reduce_sub_computation | reduce | bytes 131074
  237.0 3.1 reshape.291
  240.1 8.9 %all-to-all-start.8 = ((bf16[32,2,512]{2,1,0:T(2,128)(2,1)}), bf16[32,2,512]{2,1,0:T(2,128)(2,1)S(1)}, u32[]{:S(2)}, u32[]{:S(2)}) async-start(bf16[32,2,512]{2,1,0:T(2,128)(2,1)} %reshape.291), calls=%async_computation.8 | async-start | bytes 131072 | tf_op jit(solution)/shard_map/all_to_all | solution.py:173
  250.5 7.4 %all-to-all-done.8 = bf16[32,2,512]{2,1,0:T(2,128)(2,1)S(1)} async-done(((bf16[32,2,512]{2,1,0:T(2,128)(2,1)}), bf16[32,2,512]{2,1,0:T(2,128)(2,1)S(1)}, u32[]{:S(2)}, u32[]{:S(2)}) %all-to-all-start.8) | async-done | bytes 65568 | tf_op jit(solution)/shard_map/all_to_all | solution.py:173
  258.7 4.6 %all-to-all-start.11 = ((bf16[32,16,512]{2,1,0:T(8,128)(2,1)}), bf16[32,16,512]{2,1,0:T(8,128)(2,1)}, u32[]{:S(2)}, u32[]{:S(2)}) async-start(bf16[32,16,512]{2,1,0:T(8,128)(2,1)} %broadcast_in_dim.46), calls=%async_computation.11 | async-start | bytes 1048576 | tf_op jit(solution)/shard_map/all_to_all | solution.py:11
  268.1 9.4 %all-to-all-done.11 = bf16[32,16,512]{2,1,0:T(8,128)(2,1)} async-done(((bf16[32,16,512]{2,1,0:T(8,128)(2,1)}), bf16[32,16,512]{2,1,0:T(8,128)(2,1)}, u32[]{:S(2)}, u32[]{:S(2)}) %all-to-all-start.11) | async-done | bytes 524320 | tf_op jit(solution)/shard_map/all_to_all | solution.py:11
  278.4 8.2 %all-to-all-start.9 = ((bf16[8,32,8,128]{3,2,1,0:T(8,128)(2,1)}), bf16[8,32,8,128]{3,2,1,0:T(8,128)(2,1)S(1)}, u32[]{:S(2)}, u32[]{:S(2)}) async-start(bf16[8,32,8,128]{3,2,1,0:T(8,128)(2,1)} %broadcast_in_dim.45), calls=%async_computation.9 | async-start | bytes 1048576 | tf_op jit(solution)/shard_map/all_to_all | solution.py:11
  288.0 8.0 %all-to-all-done.9 = bf16[8,32,8,128]{3,2,1,0:T(8,128)(2,1)S(1)} async-done(((bf16[8,32,8,128]{3,2,1,0:T(8,128)(2,1)}), bf16[8,32,8,128]{3,2,1,0:T(8,128)(2,1)S(1)}, u32[]{:S(2)}, u32[]{:S(2)}) %all-to-all-start.9) | async-done | bytes 524320 | tf_op jit(solution)/shard_map/all_to_all | solution.py:11
  297.1 4.4 %all-to-all-start.12 = ((bf16[8,512,128]{2,1,0:T(8,128)(2,1)}), bf16[8,512,128]{2,1,0:T(8,128)(2,1)S(1)}, u32[]{:S(2)}, u32[]{:S(2)}) async-start(bf16[8,512,128]{2,1,0:T(8,128)(2,1)} %broadcast_in_dim.47), calls=%async_computation.12 | async-start | bytes 2097152 | tf_op jit(solution)/shard_map/all_to_all | solution.py:11
  303.2 3.2 %gather_fusion.1 = bf16[1024,128]{1,0:T(8,128)(2,1)S(1)} fusion(bf16[2048,128]{1,0:T(8,128)(2,1)S(1)} %bitcast.108, s32[1024]{0:T(1024)S(1)} %broadcast_clamp_fusion), kind=kCustom, calls=%fused_computation.1 | custom fusion | bytes 528384 | tf_op jit(solution)/shard_map/gather | solution.py:175
  306.4 3.7 %fusion.20 = f32[512,128]{1,0:T(8,128)S(1)} fusion(bf16[512,2,128]{2,1,0:T(2,128)(2,1)S(1)} %bitcast.116, f32[512,2]{1,0:T(8,128)} %copy.93), kind=kLoop, calls=%fused_computation.25 | loop fusion | flops 327680 | bytes 528384 | tf_op jit(solution)/shard_map/reduce_sum | solution.py:180
  310.1 6.4 %all-to-all-done.12 = bf16[8,512,128]{2,1,0:T(8,128)(2,1)S(1)} async-done(((bf16[8,512,128]{2,1,0:T(8,128)(2,1)}), bf16[8,512,128]{2,1,0:T(8,128)(2,1)S(1)}, u32[]{:S(2)}, u32[]{:S(2)}) %all-to-all-start.12) | async-done | bytes 1048608 | tf_op jit(solution)/shard_map/all_to_all | solution.py:11
  (98 shorter events, 35.0 us)
Async XLA Ops:
  0.6 188.4 %copy-start = (bf16[1,128,4096]{2,1,0:T(8,128)(2,1)S(1)}, bf16[1,128,4096]{2,1,0:T(8,128)(2,1)}, u32[]{:S(2)}) copy-start(bf16[1,128,4096]{2,1,0:T(8,128)(2,1)} %param.37) | copy-start | bytes 3145732
  24.5 18.8 %all-to-all-start.1 = ((bf16[32,16,512]{2,1,0:T(8,128)(2,1)}), bf16[32,16,512]{2,1,0:T(8,128)(2,1)S(1)}, u32[]{:S(2)}, u32[]{:S(2)}) async-start(bf16[32,16,512]{2,1,0:T(8,128)(2,1)} %bitcast), calls=%async_computation.1 | async-start | bytes 1048576 | tf_op jit(solution)/shard_map/all_to_all | solution.py:26
  46.8 43.6 %copy-start.7 = (f32[256]{0:T(256)S(1)}, f32[256]{0:T(256)}, u32[]{:S(2)}) copy-start(f32[256]{0:T(256)} %param.31) | copy-start | bytes 3076
  46.8 50.8 %copy-start.5 = (s32[512,2]{0,1:T(2,128)S(1)}, s32[512,2]{0,1:T(2,128)}, u32[]{:S(2)}) copy-start(s32[512,2]{0,1:T(2,128)} %param.33) | copy-start | bytes 12292
  46.9 61.1 %copy-start.4 = (bf16[256,128]{1,0:T(8,128)(2,1)S(1)}, bf16[256,128]{1,0:T(8,128)(2,1)}, u32[]{:S(2)}) copy-start(bf16[256,128]{1,0:T(8,128)(2,1)} %param.30) | copy-start | bytes 196612
  90.5 42.2 %copy-start.1 = (bf16[512,128]{1,0:T(8,128)(2,1)S(1)}, bf16[512,128]{1,0:T(8,128)(2,1)}, u32[]{:S(2)}) copy-start(bf16[512,128]{1,0:T(8,128)(2,1)} %param.21) | copy-start | bytes 393220
  91.3 55.1 %copy-start.8 = (f32[128]{0:T(128)S(1)}, f32[128]{0:T(128)}, u32[]{:S(2)}) copy-start(f32[128]{0:T(128)} %param.32) | copy-start | bytes 1540
  91.3 16.7 %all-to-all-start.2 = ((bf16[32,16,256]{2,1,0:T(8,128)(2,1)}), bf16[32,16,256]{2,1,0:T(8,128)(2,1)S(1)}, u32[]{:S(2)}, u32[]{:S(2)}) async-start(bf16[32,16,256]{2,1,0:T(8,128)(2,1)} %broadcast_in_dim.39), calls=%async_computation.2 | async-start | bytes 524288 | tf_op jit(solution)/shard_map/all_to_all | solution.py:11
  109.4 23.2 %all-to-all-start.3 = ((bf16[8,512,128]{2,1,0:T(8,128)(2,1)}), bf16[8,512,128]{2,1,0:T(8,128)(2,1)S(1)}, u32[]{:S(2)}, u32[]{:S(2)}) async-start(bf16[8,512,128]{2,1,0:T(8,128)(2,1)} %broadcast_in_dim.40), calls=%async_computation.3 | async-start | bytes 2097152 | tf_op jit(solution)/shard_map/all_to_all | solution.py:11
  133.5 12.7 %all-to-all-start.4 = ((f32[32,1,512]{2,1,0:T(1,128)}), f32[32,1,512]{2,1,0:T(1,128)S(1)}, u32[]{:S(2)}, u32[]{:S(2)}) async-start(f32[32,1,512]{2,1,0:T(1,128)} %broadcast_in_dim.41), calls=%async_computation.4 | async-start | bytes 131072 | tf_op jit(solution)/shard_map/all_to_all | solution.py:11
  170.7 25.8 %copy-start.2 = (bf16[128,512]{1,0:T(8,128)(2,1)S(1)}, bf16[128,512]{1,0:T(8,128)(2,1)}, u32[]{:S(2)}) copy-start(bf16[128,512]{1,0:T(8,128)(2,1)} %param.39) | copy-start | bytes 393220
  170.7 25.8 %copy-start.3 = (bf16[128,512]{1,0:T(8,128)(2,1)S(1)}, bf16[128,512]{1,0:T(8,128)(2,1)}, u32[]{:S(2)}) copy-start(bf16[128,512]{1,0:T(8,128)(2,1)} %param.38) | copy-start | bytes 393220
  192.1 13.8 %all-to-all-start.7 = ((bf16[8,1,8,4096]{3,2,1,0:T(8,128)(2,1)}), bf16[8,1,8,4096]{3,2,1,0:T(8,128)(2,1)S(1)}, u32[]{:S(2)}, u32[]{:S(2)}) async-start(bf16[8,1,8,4096]{3,2,1,0:T(8,128)(2,1)} %fusion), calls=%async_computation.7 | async-start | bytes 1048576 | tf_op jit(solution)/shard_map/all_to_all | solution.py:26
  205.9 34.3 %all-to-all-start.10 = ((bf16[32,16,1024]{2,1,0:T(8,128)(2,1)}), bf16[32,16,1024]{2,1,0:T(8,128)(2,1)}, u32[]{:S(2)}, u32[]{:S(2)}) async-start(bf16[32,16,1024]{2,1,0:T(8,128)(2,1)} %bitcast.28), calls=%async_computation.10 | async-start | bytes 2097152 | tf_op jit(solution)/shard_map/all_to_all | solution.py:26
  240.1 17.8 %all-to-all-start.8 = ((bf16[32,2,512]{2,1,0:T(2,128)(2,1)}), bf16[32,2,512]{2,1,0:T(2,128)(2,1)S(1)}, u32[]{:S(2)}, u32[]{:S(2)}) async-start(bf16[32,2,512]{2,1,0:T(2,128)(2,1)} %reshape.291), calls=%async_computation.8 | async-start | bytes 131072 | tf_op jit(solution)/shard_map/all_to_all | solution.py:173
  258.7 18.8 %all-to-all-start.11 = ((bf16[32,16,512]{2,1,0:T(8,128)(2,1)}), bf16[32,16,512]{2,1,0:T(8,128)(2,1)}, u32[]{:S(2)}, u32[]{:S(2)}) async-start(bf16[32,16,512]{2,1,0:T(8,128)(2,1)} %broadcast_in_dim.46), calls=%async_computation.11 | async-start | bytes 1048576 | tf_op jit(solution)/shard_map/all_to_all | solution.py:11
  266.2 35.4 %copy-start.6 = (f32[512,2]{0,1:T(2,128)S(1)}, f32[512,2]{0,1:T(2,128)}, u32[]{:S(2)}) copy-start(f32[512,2]{0,1:T(2,128)} %param.34) | copy-start | bytes 12292
  278.4 17.6 %all-to-all-start.9 = ((bf16[8,32,8,128]{3,2,1,0:T(8,128)(2,1)}), bf16[8,32,8,128]{3,2,1,0:T(8,128)(2,1)S(1)}, u32[]{:S(2)}, u32[]{:S(2)}) async-start(bf16[8,32,8,128]{3,2,1,0:T(8,128)(2,1)} %broadcast_in_dim.45), calls=%async_computation.9 | async-start | bytes 1048576 | tf_op jit(solution)/shard_map/all_to_all | solution.py:11
  287.9 28.7 %copy-start.9 = (f32[128]{0:T(128)S(1)}, f32[128]{0:T(128)}, u32[]{:S(2)}) copy-start(f32[128]{0:T(128)} %param.41) | copy-start | bytes 1540
  297.1 19.4 %all-to-all-start.12 = ((bf16[8,512,128]{2,1,0:T(8,128)(2,1)}), bf16[8,512,128]{2,1,0:T(8,128)(2,1)S(1)}, u32[]{:S(2)}, u32[]{:S(2)}) async-start(bf16[8,512,128]{2,1,0:T(8,128)(2,1)} %broadcast_in_dim.47), calls=%async_computation.12 | async-start | bytes 2097152 | tf_op jit(solution)/shard_map/all_to_all | solution.py:11
